TPU v7x, 512 devices: a 8x2x16 block of a 8x16x16 slice. The times are simulated.
512 devices in a mesh: grp: 2 (over y), ep: 16 (over z), tp: 16 (over x, core).
Axes of the slice: x: 8, y: 2, z: 16, core: 2. Of those that a mesh axis runs over, the one named last changes fastest.
The devices are a block of a 8x16x16 slice.
Arguments:
- tokens: bfloat16 [1024, 2048], P(('grp', 'ep'), 'tp'), parts along dimension 0, may hold values from -6 to 6
- gain: float32 [2048], replicated, may hold values from 0.1 to 1.9
- routes: int32 [1024, 4], P(('grp', 'ep')), parts along dimension 0, may hold values from 0 to 15, all different within a row; in each aligned block of 32 rows (0 to 31, 32 to 63, ...) at most 16 rows name the same one
- weights: float32 [1024, 4], P(('grp', 'ep')), parts along dimension 0, may hold values from 0.05 to 1
- w_gate: bfloat16 [16, 2048, 6144], P('ep', None, 'tp'), may hold values from -0.125 to 0.125
- w_up: bfloat16 [16, 2048, 6144], P('ep', None, 'tp'), may hold values from -0.125 to 0.125
- w_down: bfloat16 [16, 6144, 2048], P('ep', 'tp'), may hold values from -0.078125 to 0.078125
Outputs:
- mixed: bfloat16 [1024, 2048], P(('grp', 'ep'), 'tp'), parts along dimension 0
There are 2 independent parts, one for each index of `grp`. A program takes and returns all parts, laid end to end along the dimension named above; an argument that names none is the same for every part. Nothing has to cross between parts.
Inputs may be any that keep to these rules, and one draw needn't show every extreme that they name: `routes`: each row names 4 different experts. Among the rows of one device no expert is named by more than 16 rows, a bound that some block reaches.
All inputs are finite; a program needn't handle non-finite values.
Results may differ from a plain program's by a relative error of at most 0.019.
Values may be sent and summed in bfloat16 or wider, within the bound.
A program may use at most 64 MiB of HBM per device.

v0:
```python
import jax
import jax.numpy as jnp
from jax import lax
from jax.sharding import PartitionSpec as P

epsilon = 1e-05


def cut_along(shard, dim, count):
    lengths = shard.shape
    tiles = shard.reshape(*lengths[:dim], count, lengths[dim] // count, *lengths[dim + 1 :])
    return jnp.moveaxis(tiles, dim, 0)


def summed_on_arrival(shard, axis, dim):
    count = lax.axis_size(axis)
    tiles = lax.all_to_all(cut_along(shard, dim, count), axis, 0, 0, tiled=True)
    return jnp.sum(tiles.astype(jnp.float32), axis=0)


def in_order(tiles, dim):
    lengths = list(tiles.shape[1:])
    lengths[dim] *= tiles.shape[0]
    return jnp.moveaxis(tiles, 0, dim).reshape(lengths)


def sent_to_all(shard, axis):
    count = lax.axis_size(axis)
    return lax.all_to_all(
        jnp.broadcast_to(shard[None], (count, *shard.shape)), axis, 0, 0, tiled=True
    )


def gathered_copies(shard, axis, dim):
    return in_order(sent_to_all(shard, axis), dim)


def normalize(values, gain):
    values = values.astype(jnp.float32)
    average = jnp.mean(values, axis=1, keepdims=True)
    spread = jnp.mean(jnp.square(values - average), axis=1, keepdims=True)
    return ((values - average) * lax.rsqrt(spread + epsilon) * gain).astype(jnp.bfloat16)


def expert_rows(chosen, gate_w, up_w, down_w):
    gate_val = jnp.dot(chosen, gate_w, preferred_element_type=jnp.float32)
    up_val = jnp.dot(chosen, up_w, preferred_element_type=jnp.float32)
    hidden = (jax.nn.silu(gate_val) * up_val).astype(jnp.bfloat16)
    partial_value = jnp.dot(hidden, down_w, preferred_element_type=jnp.float32).astype(jnp.bfloat16)
    return summed_on_arrival(partial_value, "tp", 1).astype(jnp.bfloat16)


def on_device(tokens, gain, routes, weights, w_gate, w_up, w_down):
    groups = lax.axis_size("ep")
    tok_rows, top_count = routes.shape
    capacity = min(tok_rows, 2 * tok_rows * top_count // groups)
    gate_w, up_w, down_w = (w_gate[0], w_up[0], w_down[0])
    whole = gathered_copies(tokens, "tp", 1)
    normed = normalize(whole, gain)
    pair_expert = routes.reshape(-1)
    pair_token = jnp.arange(tok_rows * top_count, dtype=jnp.int32) // top_count
    member = (pair_expert[:, None] == jnp.arange(groups, dtype=jnp.int32)[None, :]).astype(
        jnp.int32
    )
    earlier = jnp.cumsum(member, axis=0) - member
    position = pair_expert * capacity + jnp.sum(earlier * member, axis=1)
    row_width = normed.shape[1]
    outbox = (
        jnp.zeros((groups * capacity, row_width), jnp.bfloat16).at[position].set(normed[pair_token])
    )
    outbox = outbox.reshape(groups, capacity, row_width)
    arrived = lax.all_to_all(outbox, "ep", split_axis=0, concat_axis=0, tiled=True)
    count = arrived.shape[1]
    flat_rows = arrived.reshape(groups * count, arrived.shape[2])
    served = expert_rows(flat_rows, gate_w, up_w, down_w).reshape(groups, count, -1)
    returned = lax.all_to_all(served, "ep", split_axis=0, concat_axis=0, tiled=True)
    picked = (
        returned.reshape(groups * capacity, -1)[position]
        .reshape(tok_rows, top_count, -1)
        .astype(jnp.float32)
    )
    return jnp.sum(picked * weights[:, :, None], axis=1).astype(jnp.bfloat16)


def solution(mesh):
    in_specs = (
        P(("grp", "ep"), "tp"),
        P(),
        P(("grp", "ep"), None),
        P(("grp", "ep"), None),
        P("ep", None, "tp"),
        P("ep", None, "tp"),
        P("ep", "tp", None),
    )
    out_specs = P(("grp", "ep"), "tp")
    return jax.shard_map(
        on_device, mesh=mesh, in_specs=in_specs, out_specs=out_specs, check_vma=False
    )
```

profile of v0, /device:TPU:80, one launch (start us, length us, event | category | flops | bytes accessed | tf_op | source)
XLA Modules:
  0.0 175.8 jit_solution(12110095106111246556)
XLA Ops:
  0.0 0.0 copy-start
  0.0 1.5 broadcast_in_dim.5
  1.5 7.6 %all-to-all-start = ((bf16[16,32,128]{2,1,0:T(8,128)(2,1)}), bf16[16,32,128]{2,1,0:T(8,128)(2,1)S(1)}, u32[]{:S(2)}, u32[]{:S(2)}) async-start(bf16[16,32,128]{2,1,0:T(8,128)(2,1)} %broadcast_in_dim.5), calls=%async_computation | async-start | bytes 262144 | tf_op jit(solution)/shard_map/all_to_all | solution.py:29
  9.1 0.8 copy.15
  9.9 0.7 broadcast_multiply_fusion
  10.6 0.1 eq.15
  10.7 0.1 fusion.31
  10.8 0.2 reduce_window_sum.11
  10.9 0.2 select_reduce_fusion
  11.1 0.1 copy.14
  11.2 0.1 mul.52
  11.3 6.2 %all-to-all-done = bf16[16,32,128]{2,1,0:T(8,128)(2,1)S(1)} async-done(((bf16[16,32,128]{2,1,0:T(8,128)(2,1)}), bf16[16,32,128]{2,1,0:T(8,128)(2,1)S(1)}, u32[]{:S(2)}, u32[]{:S(2)}) %all-to-all-start) | async-done | bytes 131104 | tf_op jit(solution)/shard_map/all_to_all | solution.py:29
  17.6 0.1 convert_reduce_fusion
  17.7 0.2 fusion.25
  17.9 0.8 fusion.28
  18.7 4.1 %scatter_custom_fusion = bf16[256,2048]{1,0:T(8,128)(2,1)} fusion(s32[128]{0:T(128)S(1)} %fusion.33, bf16[32,2048]{1,0:T(8,128)(2,1)S(1)} %fusion.28, s32[1024]{0:T(1024)S(1)} %pad_clamp_fusion.1, bf16[]{:T(256)} %constant.31.clone.1), kind=kCustom, calls=%fused_computation.13 | custom fusion | bytes 1048578 | tf_op jit(solution)/shard_map/scatter | solution.py:69
  22.8 0.0 copy-start.1
  22.8 95.3 %all_to_all.20 = bf16[16,16,2048]{2,1,0:T(8,128)(2,1)S(1)} all-to-all(bf16[16,16,2048]{2,1,0:T(8,128)(2,1)} %bitcast.55), channel_id=1, replica_groups=mesh['grp'=2,'ep'=16,'tp'=16] {'ep'}, dimensions={0} | all-to-all | bytes 2097152 | tf_op jit(solution)/shard_map/all_to_all | solution.py:72
  118.1 0.0 copy-done.1
  118.1 0.7 fusion.3
  118.9 0.0 copy-done
  118.9 3.8 %fusion.5 = bf16[32,16,8,128]{3,2,1,0:T(8,128)(2,1)} fusion(bf16[1,384,2048]{2,1,0:T(8,128)(2,1)S(1)} %copy-done, bf16[256,2048]{1,0:T(8,128)(2,1)S(1)} %bitcast.54, bf16[1,2048,384]{2,1,0:T(8,128)(2,1)} %param.12, f32[256,384]{1,0:T(8,128)S(1)} %fusion.3), kind=kOutput, calls=%fused_computation.9 | convolution fusion | flops 806420480 | bytes 5636096 | tf_op jit(solution)/shard_map/dot_general | solution.py:49
  122.7 1.5 copy.23
  124.1 0.0 copy-start.2
  124.2 30.3 %all_to_all.21 = bf16[16,256,128]{2,1,0:T(8,128)(2,1)S(1)} all-to-all(bf16[16,256,128]{2,1,0:T(8,128)(2,1)S(1)} %bitcast.56), channel_id=1, replica_groups=mesh['grp'=2,'ep'=16,'tp'=16] {'tp'}, dimensions={0} | all-to-all | bytes 2097152 | tf_op jit(solution)/shard_map/all_to_all | solution.py:17
  154.4 0.8 reduce_sum.54
  155.2 6.9 %all-to-all-start.3 = ((bf16[16,16,128]{2,1,0:T(8,128)(2,1)}), bf16[16,16,128]{2,1,0:T(8,128)(2,1)S(1)}, u32[]{:S(2)}, u32[]{:S(2)}) async-start(bf16[16,16,128]{2,1,0:T(8,128)(2,1)} %bitcast.10), calls=%async_computation.3 | async-start | bytes 131072 | tf_op jit(solution)/shard_map/all_to_all | solution.py:76
  162.0 0.0 copy-done.2
  162.0 0.1 copy.18
  162.1 12.2 %all-to-all-done.3 = bf16[16,16,128]{2,1,0:T(8,128)(2,1)S(1)} async-done(((bf16[16,16,128]{2,1,0:T(8,128)(2,1)}), bf16[16,16,128]{2,1,0:T(8,128)(2,1)S(1)}, u32[]{:S(2)}, u32[]{:S(2)}) %all-to-all-start.3) | async-done | bytes 65568 | tf_op jit(solution)/shard_map/all_to_all | solution.py:76
  174.4 0.7 gather_fusion
  175.1 0.7 fusion.30
  (6 shorter events, 0.0 us)
Async XLA Ops:
  0.0 118.9 %copy-start = (bf16[1,384,2048]{2,1,0:T(8,128)(2,1)S(1)}, bf16[1,384,2048]{2,1,0:T(8,128)(2,1)}, u32[]{:S(2)}) copy-start(bf16[1,384,2048]{2,1,0:T(8,128)(2,1)} %param.13) | copy-start | bytes 4718596
  1.5 16.1 %all-to-all-start = ((bf16[16,32,128]{2,1,0:T(8,128)(2,1)}), bf16[16,32,128]{2,1,0:T(8,128)(2,1)S(1)}, u32[]{:S(2)}, u32[]{:S(2)}) async-start(bf16[16,32,128]{2,1,0:T(8,128)(2,1)} %broadcast_in_dim.5), calls=%async_computation | async-start | bytes 262144 | tf_op jit(solution)/shard_map/all_to_all | solution.py:29
  22.8 95.3 %copy-start.1 = (bf16[1,2048,384]{2,1,0:T(8,128)(2,1)S(1)}, bf16[1,2048,384]{2,1,0:T(8,128)(2,1)}, u32[]{:S(2)}) copy-start(bf16[1,2048,384]{2,1,0:T(8,128)(2,1)} %param.11) | copy-start | bytes 4718596
  124.1 37.9 %copy-start.2 = (f32[32,4]{0,1:T(4,128)S(1)}, f32[32,4]{0,1:T(4,128)}, u32[]{:S(2)}) copy-start(f32[32,4]{0,1:T(4,128)} %param.10) | copy-start | bytes 1540
  155.2 19.2 %all-to-all-start.3 = ((bf16[16,16,128]{2,1,0:T(8,128)(2,1)}), bf16[16,16,128]{2,1,0:T(8,128)(2,1)S(1)}, u32[]{:S(2)}, u32[]{:S(2)}) async-start(bf16[16,16,128]{2,1,0:T(8,128)(2,1)} %bitcast.10), calls=%async_computation.3 | async-start | bytes 131072 | tf_op jit(solution)/shard_map/all_to_all | solution.py:76
where the time goes:
time: 178 us; the launch traced here: 176 us
  blocking collectives  126 us (71%)
  waiting for transfers between devices  18.4 us (10%)
  starting transfers between devices  14.5 us (8%)
  local copies, waits for them, and re-layouts  8.93 us (5%)
  matrix products  4.51 us (3%)
  other arithmetic  3.79 us (2%)
    all_to_all x1, blocking collectives, on_device(): lax.all_to_all(outbox, 'ep', split_axis=0, concat_axis=0, tiled=True)  95.3 us
    all_to_all x1, blocking collectives, summed_on_arrival(): tiles = lax.all_to_all(cut_along(shard, dim, count), axis, 0, 0, tiled=True)  30.3 us
    all_to_all x1, waiting for transfers between devices, on_device(): lax.all_to_all(served, 'ep', split_axis=0, concat_axis=0, tiled=True)  12.2 us
    all_to_all x1, starting transfers between devices, sent_to_all(): lax.all_to_all(jnp.broadcast_to(shard[None], (count, *shard.shape)), axis...  7.63 us
    all_to_all x1, starting transfers between devices, on_device(): lax.all_to_all(served, 'ep', split_axis=0, concat_axis=0, tiled=True)  6.85 us
    all_to_all x1, waiting for transfers between devices, sent_to_all(): lax.all_to_all(jnp.broadcast_to(shard[None], (count, *shard.shape)), axis...  6.21 us
    scatter x1, local copies, waits for them, and re-layouts, on_device(): jnp.zeros((groups * capacity, row_width), jnp.bfloat16).at[position]  4.11 us
    dot_general x1, matrix products, expert_rows(): jnp.dot(hidden, down_w, preferred_element_type=jnp.float32)  3.78 us
  transfers between devices with their start and end apart: 2, of which 2 were waited for; matrix products, arithmetic and copies ran while one was open for 1% of the time, Pallas kernels for 0%

commit v1 on v0

v1 whole, which is shorter than its diff:
```python
import functools

import jax
import jax.numpy as jnp
from jax import lax
from jax.experimental import pallas as pl
from jax.experimental.pallas import tpu as pltpu
from jax.sharding import PartitionSpec as P

MESH = pl.DeviceIdType.MESH
epsilon = 1e-05
CHIPS = 8
CHUNKS = 2


def ring_offsets(count):
    offsets = [0]
    for distance in range(1, count // 2):
        offsets += [distance, -distance]
    return offsets + [count // 2]


def kernel(
    n_ep, cap,
    tok_hbm, gain_hbm, routes_hbm, weights_hbm, wg_hbm, wu_hbm, wd_hbm,
    out_ref,
    tok, gain, routes, weights, w_in, w_own, w_other,
    packed, gathered, rows_in, part_own, part_out, part_in, sums_out, sums_in, served, returned,
    small_sem, in_sem, own_sem, other_sem,
    z_send, z_recv, ag_send, ag_recv, d2d_send, d2d_recv, half_send, half_recv,
    rs_send, rs_recv, back_send, back_recv,
):
    z = lax.axis_index("ep")
    tp = lax.axis_index("tp")
    core = lax.rem(tp, 2)
    x = lax.div(tp, 2)
    tok_rows, width = tok.shape
    top = routes.shape[0]
    hidden_units = w_own.shape[0]
    offsets = ring_offsets(n_ep)
    all_rows = n_ep * cap
    rows = all_rows // CHUNKS
    half = rows // 2
    slots = n_ep // CHUNKS

    def chip(d):
        return lax.rem(x + d, CHIPS)

    def at_chip(d):
        return {"tp": chip(d) * 2 + core}

    def ring(offset):
        return lax.rem(z + offset + n_ep, n_ep)

    sibling = {"tp": x * 2 + 1 - core}

    def owner(p, d):
        return chip(d) * 2 + (core if p == 0 else 1 - core)

    barrier = pltpu.get_barrier_semaphore()
    for offset in offsets[:0:-1]:
        pl.semaphore_signal(barrier, inc=1, device_id={"ep": ring(offset)}, device_id_type=MESH)
    for d in (2, 6, 1, 7):
        pl.semaphore_signal(barrier, inc=1, device_id=at_chip(d), device_id_type=MESH)
    pl.semaphore_signal(barrier, inc=1, device_id=sibling, device_id_type=MESH)

    small = [
        pltpu.make_async_copy(source, target, small_sem.at[i])
        for i, (source, target) in enumerate(
            [(tok_hbm, tok), (routes_hbm, routes), (weights_hbm, weights), (gain_hbm, gain)]
        )
    ]
    for copy in small:
        copy.start()
    for p in range(2):
        for d in range(CHIPS):
            first = pl.multiple_of(owner(p, d) * width, width)
            k = p * CHIPS + d
            for j, source in enumerate((wg_hbm, wu_hbm)):
                pltpu.make_async_copy(
                    source.at[0, pl.ds(first, width), :],
                    w_in.at[pl.ds(k * width, width), pl.ds(j * hidden_units, hidden_units)],
                    in_sem,
                ).start()
    for p, target, sem in ((1, w_other, other_sem), (0, w_own, own_sem)):
        for d in range(CHIPS):
            first = pl.multiple_of(owner(p, d) * width, width)
            pltpu.make_async_copy(
                wd_hbm.at[0, :, pl.ds(first, width)], target.at[:, pl.ds(d * width, width)], sem
            ).start()

    small[0].wait()
    small[1].wait()
    place = lax.broadcasted_iota(jnp.int32, (all_rows, tok_rows), 0)
    place_expert = lax.div(place, cap)
    place_turn = lax.rem(place, cap)
    hits = [
        (jnp.broadcast_to(routes[k : k + 1, :], (all_rows, tok_rows)) == place_expert)
        for k in range(top)
    ]
    member = sum(hit.astype(jnp.float32) for hit in hits)
    earlier = (
        lax.broadcasted_iota(jnp.int32, (tok_rows, tok_rows), 0)
        < lax.broadcasted_iota(jnp.int32, (tok_rows, tok_rows), 1)
    ).astype(jnp.float32).astype(jnp.bfloat16)
    turn = jnp.dot(member.astype(jnp.bfloat16), earlier, preferred_element_type=jnp.float32)
    chosen = jnp.where(turn == place_turn.astype(jnp.float32), member, 0.0)
    outbox = jnp.dot(
        chosen.astype(jnp.bfloat16), tok[...], preferred_element_type=jnp.float32
    ).astype(jnp.bfloat16)
    packed[...] = outbox.reshape(n_ep, cap, width)

    pl.semaphore_wait(barrier, (n_ep - 1) + 4 + 1)

    sent = []

    def send(src, dst, send_sem, recv_sem, device):
        copy = pltpu.make_async_remote_copy(
            src_ref=src, dst_ref=dst, send_sem=send_sem, recv_sem=recv_sem,
            device_id=device, device_id_type=MESH,
        )
        copy.start()
        sent.append(copy)
        return copy

    def slot_rows(i):
        return pl.ds(i * cap, cap)

    dispatch = {}
    for i in range(n_ep - 1, 0, -1):
        expert = ring(-offsets[i])
        dispatch[i] = send(
            packed.at[expert], gathered.at[0, 0, slot_rows(i), :], z_send.at[i], z_recv.at[i],
            {"ep": expert},
        )
    gathered[0, 0, 0:cap, :] = packed[z]

    small[2].wait()
    mix = sum(
        jnp.where(hit, jnp.broadcast_to(weights[k : k + 1, :], (all_rows, tok_rows)), 0.0)
        for k, hit in enumerate(hits)
    ) * chosen
    mix_high = mix.astype(jnp.bfloat16)
    mix_low = (mix - mix_high.astype(jnp.float32)).astype(jnp.bfloat16)
    unit = (
        lax.broadcasted_iota(jnp.int32, (tok_rows, tok_rows), 0)
        == lax.broadcasted_iota(jnp.int32, (tok_rows, tok_rows), 1)
    ).astype(jnp.float32).astype(jnp.bfloat16)

    def flipped(value):
        return lax.dot_general(
            unit, value, (((1,), (1,)), ((), ())), preferred_element_type=jnp.float32
        ).astype(jnp.bfloat16)

    mix_high, mix_low = flipped(mix_high), flipped(mix_low)

    def span(c):
        return pl.ds(c * rows, rows)

    def top_half(c):
        return pl.ds(c * rows, half)

    def low_half(c):
        return pl.ds(c * rows + half, half)

    ag, d2d, halves, rs, back = {}, {}, {}, {}, {}

    def to_sibling(c, d, at, kind):
        d2d[c, kind] = send(
            gathered.at[0, d, at, :], gathered.at[1, d, at, :],
            d2d_send.at[c, kind], d2d_recv.at[c, kind], sibling,
        )

    def gather_own(c):
        for i in range(max(1, c * slots), (c + 1) * slots):
            dispatch[i].wait_recv()
        for kind, d, slot in ((2, 6, 2), (6, 2, 6), (1, 7, 1), (7, 1, 7)):
            ag[c, kind] = send(
                gathered.at[0, 0, span(c), :], gathered.at[0, slot, span(c), :],
                ag_send.at[c, kind], ag_recv.at[c, kind], at_chip(d),
            )
        to_sibling(c, 0, span(c), 0)

    def gather_relay(c):
        for slot, near, far, opposite, at, kind in (
            (2, 7, 6, 3, top_half(c), 4),
            (6, 1, 2, 5, low_half(c), 0),
        ):
            ag[c, slot].wait_recv()
            ag[c, kind] = send(
                gathered.at[0, slot, at, :], gathered.at[0, 4, at, :],
                ag_send.at[c, kind], ag_recv.at[c, kind], at_chip(far),
            )
            ag[c, opposite] = send(
                gathered.at[0, slot, span(c), :], gathered.at[0, opposite, span(c), :],
                ag_send.at[c, opposite], ag_recv.at[c, opposite], at_chip(near),
            )
            to_sibling(c, slot, span(c), slot)
        for slot in (1, 7):
            ag[c, slot].wait_recv()
            to_sibling(c, slot, span(c), slot)

    def gather_last(c):
        for slot in (3, 5):
            ag[c, slot].wait_recv()
            to_sibling(c, slot, span(c), slot)
        ag[c, 4].wait_recv()
        to_sibling(c, 4, top_half(c), 4)
        ag[c, 0].wait_recv()
        to_sibling(c, 4, low_half(c), 8)

    def feed(c):
        for kind in range(9):
            d2d[c, kind].wait_recv()
        blocks = [(p, d) for p in range(2) for d in range(CHIPS)]
        features = len(blocks) * width
        total = jnp.zeros((rows, width), jnp.float32)
        for p, d in blocks:
            total += gathered[p, d, span(c), :].astype(jnp.float32)
        average = jnp.sum(total, axis=1, keepdims=True) / features
        total = jnp.zeros((rows, width), jnp.float32)
        for p, d in blocks:
            off = gathered[p, d, span(c), :].astype(jnp.float32) - average
            total += off * off
        scale = lax.rsqrt(jnp.sum(total, axis=1, keepdims=True) / features + epsilon)
        for p, d in blocks:
            k = p * CHIPS + d
            off = gathered[p, d, span(c), :].astype(jnp.float32) - average
            rows_in[span(c), pl.ds(k * width, width)] = (
                off * scale * gain[pl.ds(owner(p, d), 1), :]
            ).astype(jnp.bfloat16)

    def expert(c):
        both = jnp.dot(rows_in[span(c), :], w_in[...], preferred_element_type=jnp.float32)
        gate_val, up_val = both[:, :hidden_units], both[:, hidden_units:]
        return (gate_val / (1.0 + jnp.exp(-gate_val)) * up_val).astype(jnp.bfloat16)

    def project(c, hidden):
        other = jnp.dot(hidden, w_other[...], preferred_element_type=jnp.float32)
        other = other.astype(jnp.bfloat16)
        for d in range(CHIPS):
            part_out[c, d] = other[:, d * width : (d + 1) * width]
        halves[c] = send(
            part_out.at[c], part_in.at[c], half_send.at[c], half_recv.at[c], sibling
        )
        part_own[c] = jnp.dot(hidden, w_own[...], preferred_element_type=jnp.float32)

    def chip_part(c, d):
        return part_own[c, :, pl.ds(d * width, width)] + part_in[c, d].astype(jnp.float32)

    def reduce_send(c, kind, d, source, slot, at=None):
        src, dst = sums_out.at[c, source], sums_in.at[c, slot]
        if at is not None:
            src, dst = src.at[at, :], dst.at[at, :]
        rs[c, kind] = send(src, dst, rs_send.at[c, kind], rs_recv.at[c, kind], at_chip(d))

    def reduce_first(c):
        halves[c].wait_recv()
        sums_out[c, 4] = chip_part(c, 4).astype(jnp.bfloat16)
        reduce_send(c, 4, 2, 4, 4, pl.ds(0, half))
        reduce_send(c, 0, 6, 4, 4, pl.ds(half, half))
        for d, near in ((3, 1), (5, 7), (1, 1), (7, 7)):
            sums_out[c, d] = chip_part(c, d).astype(jnp.bfloat16)
            reduce_send(c, d, near, d, d)

    def reduce_second(c):
        rs[c, 4].wait_recv()
        rs[c, 0].wait_recv()
        for d, near, at in ((2, 3, 0), (6, 5, half)):
            rs[c, near].wait_recv()
            value = chip_part(c, d) + sums_in[c, near].astype(jnp.float32)
            sums_out[c, d] = value.astype(jnp.bfloat16)
            sums_out[c, d, pl.ds(at, half), :] = (
                value[at : at + half] + sums_in[c, 4, pl.ds(at, half), :].astype(jnp.float32)
            ).astype(jnp.bfloat16)
            reduce_send(c, d, d, d, d)

    def finish(c):
        value = chip_part(c, 0)
        for slot in (1, 7, 2, 6):
            rs[c, slot].wait_recv()
            value += sums_in[c, slot].astype(jnp.float32)
        served[span(c), :] = value.astype(jnp.bfloat16)
        for i in range((c + 1) * slots - 1, max(1, c * slots) - 1, -1):
            back[i] = send(
                served.at[slot_rows(i), :], returned.at[z], back_send.at[i], back_recv.at[i],
                {"ep": ring(offsets[i])},
            )
        if c == 0:
            returned[z] = served[0:cap, :]

    gather_own(0)
    gather_own(1)
    gather_relay(0)
    gather_relay(1)
    gather_last(0)
    small[3].wait()
    feed(0)
    pltpu.make_async_copy(w_in, w_in, in_sem).wait()
    hidden = expert(0)
    pltpu.make_async_copy(w_other, w_other, other_sem).wait()
    pltpu.make_async_copy(w_own, w_own, own_sem).wait()
    project(0, hidden)
    gather_last(1)
    reduce_first(0)
    feed(1)
    project(1, expert(1))
    reduce_second(0)
    reduce_first(1)
    finish(0)
    reduce_second(1)
    finish(1)

    for i in range(n_ep - 1, 0, -1):
        back[i].wait_recv()
    values = returned[...].reshape(all_rows, width)
    out_ref[...] = (
        jnp.dot(mix_high, values, preferred_element_type=jnp.float32)
        + jnp.dot(mix_low, values, preferred_element_type=jnp.float32)
    ).astype(out_ref.dtype)
    for copy in sent:
        copy.wait_send()


def solution(mesh):
    n_ep, n_tp = mesh.shape["ep"], mesh.shape["tp"]

    def on_device(tokens, gain, routes, weights, w_gate, w_up, w_down):
        tok_rows, width = tokens.shape
        top = routes.shape[1]
        cap = min(tok_rows, 2 * tok_rows * top // n_ep)
        hidden_units = w_gate.shape[2]
        all_rows = n_ep * cap
        rows = all_rows // CHUNKS
        features = n_tp * width
        bf16, f32 = jnp.bfloat16, jnp.float32
        dma = pltpu.SemaphoreType.DMA
        return pl.pallas_call(
            functools.partial(kernel, n_ep, cap),
            out_shape=jax.ShapeDtypeStruct((tok_rows, width), bf16),
            in_specs=[pl.BlockSpec(memory_space=pltpu.HBM)] * 7,
            out_specs=pl.BlockSpec(memory_space=pltpu.VMEM),
            scratch_shapes=[
                pltpu.VMEM((tok_rows, width), bf16),
                pltpu.VMEM((n_tp, width), f32),
                pltpu.VMEM((top, tok_rows), jnp.int32),
                pltpu.VMEM((top, tok_rows), f32),
                pltpu.VMEM((features, 2 * hidden_units), bf16),
                pltpu.VMEM((hidden_units, features // 2), bf16),
                pltpu.VMEM((hidden_units, features // 2), bf16),
                pltpu.VMEM((n_ep, cap, width), bf16),
                pltpu.VMEM((2, CHIPS, all_rows, width), bf16),
                pltpu.VMEM((all_rows, features), bf16),
                pltpu.VMEM((CHUNKS, rows, features // 2), f32),
                pltpu.VMEM((CHUNKS, CHIPS, rows, width), bf16),
                pltpu.VMEM((CHUNKS, CHIPS, rows, width), bf16),
                pltpu.VMEM((CHUNKS, CHIPS, rows, width), bf16),
                pltpu.VMEM((CHUNKS, CHIPS, rows, width), bf16),
                pltpu.VMEM((all_rows, width), bf16),
                pltpu.VMEM((n_ep, cap, width), bf16),
                dma((4,)), dma, dma, dma,
                dma((n_ep,)), dma((n_ep,)),
                dma((CHUNKS, 8)), dma((CHUNKS, 8)),
                dma((CHUNKS, 9)), dma((CHUNKS, 9)),
                dma((CHUNKS,)), dma((CHUNKS,)),
                dma((CHUNKS, 8)), dma((CHUNKS, 8)),
                dma((n_ep,)), dma((n_ep,)),
            ],
            compiler_params=pltpu.CompilerParams(collective_id=0, has_side_effects=True),
        )(tokens, gain.reshape(n_tp, width), routes.T, weights.T, w_gate, w_up, w_down)

    in_specs = (
        P(("grp", "ep"), "tp"),
        P(),
        P(("grp", "ep"), None),
        P(("grp", "ep"), None),
        P("ep", None, "tp"),
        P("ep", None, "tp"),
        P("ep", "tp", None),
    )
    out_specs = P(("grp", "ep"), "tp")
    return jax.shard_map(
        on_device, mesh=mesh, in_specs=in_specs, out_specs=out_specs, check_vma=False
    )
```

time: 178 us -> 89.5 us (0.50); the launches traced: 176 us -> 89.3 us
  blocking collectives: 126 us -> 0 us
  Pallas kernels: 0 us -> 88 us
  waiting for transfers between devices: 18.4 us -> 0 us
  starting transfers between devices: 14.5 us -> 0 us
  local copies, waits for them, and re-layouts: 8.93 us -> 1.3 us
  matrix products: 4.51 us -> 0 us
  other arithmetic: 3.79 us -> 0 us
    all_to_all x2 -> x0, blocking collectives: 126 us -> none  [the longest x1 95.3 us: on_device(): lax.all_to_all(outbox, 'ep', split_axis=0, concat_axis=0, tiled=True)]
    pallas_call x0 -> x1, Pallas kernels: none -> 88 us  [on_device(): pl.pallas_call(functools.partial(kernel, n_ep, cap), out_shape=jax.ShapeD...]
    all_to_all x2 -> x0, waiting for transfers between devices: 18.4 us -> none  [the longest x1 12.2 us: on_device(): lax.all_to_all(served, 'ep', split_axis=0, concat_axis=0, tiled=True)]
    all_to_all x2 -> x0, starting transfers between devices: 14.5 us -> none  [the longest x1 7.63 us: sent_to_all(): lax.all_to_all(jnp.broadcast_to(shard[None], (count, *shard.shape)), axis...]
    dot_general x2 -> x0, matrix products: 4.51 us -> none  [the longest x1 3.78 us: expert_rows(): jnp.dot(hidden, down_w, preferred_element_type=jnp.float32)]
    scatter x1 -> x0, local copies, waits for them, and re-layouts: 4.11 us -> none  [on_device(): jnp.zeros((groups * capacity, row_width), jnp.bfloat16).at[position]]
    reduce_sum x5 -> x0, other arithmetic: 2 us -> none  [the longest x1 0.76 us: summed_on_arrival(): return jnp.sum(tiles.astype(jnp.float32), axis=0)]
  transfers between devices with their start and end apart: 2 -> 0, of which waited for: 2 -> 0; matrix products, arithmetic and copies ran while one was open for 1% -> 0% of each run, Pallas kernels for 0% -> 0%
where the time goes in v1:
time: 89.5 us; the launch traced here: 89.3 us
  Pallas kernels  88 us (98%)
  local copies, waits for them, and re-layouts  1.3 us (1%)
    pallas_call x1, Pallas kernels, on_device(): pl.pallas_call(functools.partial(kernel, n_ep, cap), out_shape=jax.ShapeD...  88 us

profile of v1, /device:TPU:80, one launch (start us, length us, event | category | flops | bytes accessed | tf_op | source)
XLA Modules:
  0.0 89.3 jit_solution(17563043676237780401)
XLA Ops:
  0.0 88.0 %shard_map.73 = bf16[32,128]{1,0:T(8,128)(2,1)} custom-call(bf16[32,128]{1,0:T(8,128)(2,1)} %tok_hbm.1, f32[16,128]{1,0:T(8,128)} %bitcast.3, s32[4,32]{1,0:T(4,128)} %bitcast.4, f32[4,32]{1,0:T(4,128)} %bitcast.5, bf16[1,2048,384]{2,1,0:T(8,128)(2,1)} %wg_hbm.1, bf16[1,2048,384]{2,1,0:T(8,128)(2,1)} %wu_hbm.1, bf16[1,384,2048]{2,1,0:T(8,128)(2,1)} %wd_hbm.1), custom_call_target="tpu_custom_call" | custom-call | tf_op jit(solution)/shard_map/pallas_call | solution.py:338
  88.0 1.3 %copy.9 = bf16[32,128]{1,0:T(8,128)(2,1)} copy(bf16[32,128]{1,0:T(8,128)(2,1)} %shard_map.73) | data formatting | bytes 16384

commit v2 on v0

v2 whole, which is shorter than its diff:
```python
import functools

import jax
import jax.numpy as jnp
from jax import lax
from jax.experimental import pallas as pl
from jax.experimental.pallas import tpu as pltpu
from jax.sharding import PartitionSpec as P

MESH = pl.DeviceIdType.MESH
epsilon = 1e-05
SOURCES = 2


def kernel(
    n_ep, chips, cap,
    tok_hbm, gain_hbm, routes_hbm, weights_hbm, wg_hbm, wu_hbm, wd_hbm,
    out_ref,
    tok, gain, routes, weights, w_in, w_own, w_other,
    packed, gathered, part_own, part_out, part_in, sums_out, sums_in, served, returned,
    small_sem, in_sem, own_sem, other_sem, ready_z, ready_x, ready_core,
    z_send, z_recv, ag_send, ag_recv, d2d_send, d2d_recv, half_send, half_recv,
    rs_send, rs_recv, back_send, back_recv,
):
    z = lax.axis_index("ep")
    tp = lax.axis_index("tp")
    core = lax.rem(tp, 2)
    x = lax.div(tp, 2)
    tok_rows, width = tok.shape
    top = routes.shape[0]
    hidden_units = w_own.shape[0]
    all_rows = n_ep * cap
    chunks = n_ep // SOURCES
    rows = SOURCES * cap
    far_first = sorted(range(1, chips), key=lambda d: -min(d, chips - d))

    def chip(d):
        return lax.rem(x + d, chips)

    def at_chip(number):
        return {"tp": number * 2 + core}

    sibling = {"tp": x * 2 + 1 - core}

    def owner(p, d):
        return chip(d) * 2 + (core if p == 0 else 1 - core)

    def each(low, high, body):
        lax.fori_loop(low, high, lambda i, carry: (body(i), carry)[1], 0)

    barrier = pltpu.get_barrier_semaphore()

    def greet(device):
        pl.semaphore_signal(barrier, inc=1, device_id=device, device_id_type=MESH)

    each(z + 1, n_ep, lambda s: greet({"ep": s}))
    each(x + 1, chips, lambda s: greet(at_chip(s)))

    @pl.when(core == 0)
    def _():
        greet(sibling)

    small = [
        pltpu.make_async_copy(source, target, small_sem.at[i])
        for i, (source, target) in enumerate(
            [(tok_hbm, tok), (routes_hbm, routes), (weights_hbm, weights), (gain_hbm, gain)]
        )
    ]
    for copy in small:
        copy.start()
    for p in range(2):
        for d in range(chips):
            first = pl.multiple_of(owner(p, d) * width, width)
            k = p * chips + d
            for j, source in enumerate((wg_hbm, wu_hbm)):
                pltpu.make_async_copy(
                    source.at[0, pl.ds(first, width), :],
                    w_in.at[pl.ds(k * width, width), pl.ds(j * hidden_units, hidden_units)],
                    in_sem,
                ).start()
    for p, target, sem in ((1, w_other, other_sem), (0, w_own, own_sem)):
        for d in range(chips):
            first = pl.multiple_of(owner(p, d) * width, width)
            pltpu.make_async_copy(
                wd_hbm.at[0, :, pl.ds(first, width)], target.at[:, pl.ds(d * width, width)], sem
            ).start()

    below = z + x + core

    @pl.when(below > 0)
    def _():
        pl.semaphore_wait(barrier, below)

    def answer(semaphore, device):
        pl.semaphore_signal(semaphore, inc=1, device_id=device, device_id_type=MESH)

    each(0, z, lambda s: answer(ready_z.at[z], {"ep": s}))
    each(0, x, lambda s: answer(ready_x.at[x], at_chip(s)))

    @pl.when(core == 1)
    def _():
        answer(ready_core, sibling)

    small[0].wait()
    small[1].wait()
    place = lax.broadcasted_iota(jnp.int32, (all_rows, tok_rows), 0)
    place_expert = lax.div(place, cap)
    place_turn = lax.rem(place, cap)
    hits = [
        (jnp.broadcast_to(routes[k : k + 1, :], (all_rows, tok_rows)) == place_expert)
        for k in range(top)
    ]
    member = sum(hit.astype(jnp.float32) for hit in hits)
    earlier = (
        lax.broadcasted_iota(jnp.int32, (tok_rows, tok_rows), 0)
        < lax.broadcasted_iota(jnp.int32, (tok_rows, tok_rows), 1)
    ).astype(jnp.float32).astype(jnp.bfloat16)
    turn = jnp.dot(member.astype(jnp.bfloat16), earlier, preferred_element_type=jnp.float32)
    chosen = jnp.where(turn == place_turn.astype(jnp.float32), member, 0.0)
    outbox = jnp.dot(
        chosen.astype(jnp.bfloat16), tok[...], preferred_element_type=jnp.float32
    ).astype(jnp.bfloat16)
    packed[...] = outbox.reshape(n_ep, cap, width)

    def remote(src, dst, send_sem, recv_sem, device):
        return pltpu.make_async_remote_copy(
            src_ref=src, dst_ref=dst, send_sem=send_sem, recv_sem=recv_sem,
            device_id=device, device_id_type=MESH,
        )

    def landed(ref, semaphore):
        pltpu.make_async_copy(ref, ref, semaphore).wait()

    def dispatch(s):
        remote(
            packed.at[s], gathered.at[0, 0, z], z_send.at[s], z_recv.at[z], {"ep": s}
        ).start()

    each(0, z, dispatch)
    gathered[0, 0, z] = packed[z]

    small[2].wait()
    mix = sum(
        jnp.where(hit, jnp.broadcast_to(weights[k : k + 1, :], (all_rows, tok_rows)), 0.0)
        for k, hit in enumerate(hits)
    ) * chosen
    mix_high = mix.astype(jnp.bfloat16)
    mix_low = (mix - mix_high.astype(jnp.float32)).astype(jnp.bfloat16)
    unit = (
        lax.broadcasted_iota(jnp.int32, (tok_rows, tok_rows), 0)
        == lax.broadcasted_iota(jnp.int32, (tok_rows, tok_rows), 1)
    ).astype(jnp.float32).astype(jnp.bfloat16)

    def flipped(value):
        return lax.dot_general(
            unit, value, (((1,), (1,)), ((), ())), preferred_element_type=jnp.float32
        ).astype(jnp.bfloat16)

    mix_high, mix_low = flipped(mix_high), flipped(mix_low)

    def span(c):
        return pl.ds(c * SOURCES, SOURCES)

    def dispatch_up(c):
        for j in range(SOURCES):
            s = c * SOURCES + j

            @pl.when(s > z)
            def _():
                pl.semaphore_wait(ready_z.at[s], 1)
                dispatch(s)

    def gather(c):
        for j in range(SOURCES):
            s = c * SOURCES + j

            @pl.when(s != z)
            def _():
                landed(gathered.at[0, 0, s], z_recv.at[s])

        for d in far_first:
            remote(
                gathered.at[0, 0, span(c)], gathered.at[0, chips - d, span(c)],
                ag_send.at[c], ag_recv.at[c], at_chip(chip(d)),
            ).start()

    def across(c):
        return remote(
            gathered.at[0, :, span(c)], gathered.at[1, :, span(c)],
            d2d_send.at[c], d2d_recv.at[c], sibling,
        )

    def share(c):
        landed(gathered.at[0, 1:, span(c)], ag_recv.at[c])
        across(c).start()

    def half(c):
        return remote(
            part_out.at[c], part_in.at[c], half_send.at[c], half_recv.at[c], sibling
        )

    def serve(c):
        across(c).wait_recv()
        blocks = [(p, d) for p in range(2) for d in range(chips)]
        features = len(blocks) * width
        values = [
            gathered[p, d, span(c)].reshape(rows, width).astype(jnp.float32) for p, d in blocks
        ]
        average = jnp.sum(sum(values), axis=1, keepdims=True) / features
        values = [value - average for value in values]
        spread = jnp.sum(sum(v * v for v in values), axis=1, keepdims=True) / features
        scale = lax.rsqrt(spread + epsilon)
        normed = [
            (value * scale * gain[pl.ds(owner(p, d), 1), :]).astype(jnp.bfloat16)
            for value, (p, d) in zip(values, blocks)
        ]
        both = jnp.dot(
            jnp.concatenate(normed, axis=1), w_in[...], preferred_element_type=jnp.float32
        )
        gate_val, up_val = both[:, :hidden_units], both[:, hidden_units:]
        hidden = (gate_val / (1.0 + jnp.exp(-gate_val)) * up_val).astype(jnp.bfloat16)
        other = jnp.dot(hidden, w_other[...], preferred_element_type=jnp.float32)
        other = other.astype(jnp.bfloat16)
        for d in range(chips):
            part_out[c, d] = other[:, d * width : (d + 1) * width]
        half(c).start()
        own = jnp.dot(hidden, w_own[...], preferred_element_type=jnp.float32)
        for d in range(chips):
            part_own[c, d] = own[:, d * width : (d + 1) * width]

    def reduce(c):
        half(c).wait_recv()
        for d in far_first:
            sums_out[c, d] = (part_own[c, d] + part_in[c, d].astype(jnp.float32)).astype(
                jnp.bfloat16
            )
            remote(
                sums_out.at[c, d], sums_in.at[c, chips - d], rs_send.at[c], rs_recv.at[c],
                at_chip(chip(d)),
            ).start()

    def back(s):
        return remote(
            served.at[s], returned.at[z], back_send.at[s], back_recv.at[z], {"ep": s}
        )

    def finish(c):
        landed(sums_in.at[c, 1:], rs_recv.at[c])
        value = part_own[c, 0] + part_in[c, 0].astype(jnp.float32)
        for d in range(1, chips):
            value += sums_in[c, d].astype(jnp.float32)
        served[span(c)] = value.astype(jnp.bfloat16).reshape(SOURCES, cap, width)
        for j in range(SOURCES):
            s = c * SOURCES + j

            @pl.when(s != z)
            def _():
                back(s).start()

            @pl.when(s == z)
            def _():
                returned[z] = served[z]

    small[3].wait()
    landed(w_in, in_sem)
    landed(w_other, other_sem)
    landed(w_own, own_sem)
    each(x + 1, chips, lambda s: pl.semaphore_wait(ready_x.at[s], 1))

    @pl.when(core == 0)
    def _():
        pl.semaphore_wait(ready_core, 1)

    dispatch_up(0)

    def step(i):
        pl.when(i + 1 < chunks)(lambda: dispatch_up(i + 1))
        pl.when(i < chunks)(lambda: gather(i))
        pl.when((i >= 2) & (i < chunks + 2))(lambda: reduce(i - 2))

        @pl.when((i >= 1) & (i < chunks + 1))
        def _():
            share(i - 1)
            serve(i - 1)

        pl.when(i >= 3)(lambda: finish(i - 3))

    each(0, chunks + 3, step)

    def others(body):
        each(0, z, body)
        each(z + 1, n_ep, body)

    others(lambda e: landed(returned.at[e], back_recv.at[e]))
    values = returned[...].reshape(all_rows, width)
    out_ref[...] = (
        jnp.dot(mix_high, values, preferred_element_type=jnp.float32)
        + jnp.dot(mix_low, values, preferred_element_type=jnp.float32)
    ).astype(out_ref.dtype)

    def settle(s):
        landed(packed.at[s], z_send.at[s])
        landed(served.at[s], back_send.at[s])

    others(settle)

    def settle_chunk(c):
        landed(gathered.at[0, 1:, span(c)], ag_send.at[c])
        across(c).wait_send()
        half(c).wait_send()
        landed(sums_out.at[c, 1:], rs_send.at[c])

    each(0, chunks, settle_chunk)


def solution(mesh):
    n_ep, n_tp = mesh.shape["ep"], mesh.shape["tp"]
    chips = n_tp // 2
    chunks = n_ep // SOURCES

    def on_device(tokens, gain, routes, weights, w_gate, w_up, w_down):
        tok_rows, width = tokens.shape
        top = routes.shape[1]
        cap = min(tok_rows, 2 * tok_rows * top // n_ep)
        hidden_units = w_gate.shape[2]
        rows = SOURCES * cap
        features = n_tp * width
        bf16, f32 = jnp.bfloat16, jnp.float32
        dma = pltpu.SemaphoreType.DMA
        regular = pltpu.SemaphoreType.REGULAR
        return pl.pallas_call(
            functools.partial(kernel, n_ep, chips, cap),
            out_shape=jax.ShapeDtypeStruct((tok_rows, width), bf16),
            in_specs=[pl.BlockSpec(memory_space=pltpu.HBM)] * 7,
            out_specs=pl.BlockSpec(memory_space=pltpu.VMEM),
            scratch_shapes=[
                pltpu.VMEM((tok_rows, width), bf16),
                pltpu.VMEM((n_tp, width), f32),
                pltpu.VMEM((top, tok_rows), jnp.int32),
                pltpu.VMEM((top, tok_rows), f32),
                pltpu.VMEM((features, 2 * hidden_units), bf16),
                pltpu.VMEM((hidden_units, features // 2), bf16),
                pltpu.VMEM((hidden_units, features // 2), bf16),
                pltpu.VMEM((n_ep, cap, width), bf16),
                pltpu.VMEM((2, chips, n_ep, cap, width), bf16),
                pltpu.VMEM((chunks, chips, rows, width), f32),
                pltpu.VMEM((chunks, chips, rows, width), bf16),
                pltpu.VMEM((chunks, chips, rows, width), bf16),
                pltpu.VMEM((chunks, chips, rows, width), bf16),
                pltpu.VMEM((chunks, chips, rows, width), bf16),
                pltpu.VMEM((n_ep, cap, width), bf16),
                pltpu.VMEM((n_ep, cap, width), bf16),
                dma((4,)), dma, dma, dma,
                regular((n_ep,)), regular((chips,)), regular,
                dma((n_ep,)), dma((n_ep,)),
                dma((chunks,)), dma((chunks,)),
                dma((chunks,)), dma((chunks,)),
                dma((chunks,)), dma((chunks,)),
                dma((chunks,)), dma((chunks,)),
                dma((n_ep,)), dma((n_ep,)),
            ],
            compiler_params=pltpu.CompilerParams(collective_id=0, has_side_effects=True),
        )(tokens, gain.reshape(n_tp, width), routes.T, weights.T, w_gate, w_up, w_down)

    in_specs = (
        P(("grp", "ep"), "tp"),
        P(),
        P(("grp", "ep"), None),
        P(("grp", "ep"), None),
        P("ep", None, "tp"),
        P("ep", None, "tp"),
        P("ep", "tp", None),
    )
    out_specs = P(("grp", "ep"), "tp")
    return jax.shard_map(
        on_device, mesh=mesh, in_specs=in_specs, out_specs=out_specs, check_vma=False
    )
```

time: 178 us -> 99.3 us (0.56)
  the two profiles are of different devices: /device:TPU:80 before, /device:TPU:65 now
where the time goes in v2:
time: 99.3 us; the launch traced here: 99.1 us
  Pallas kernels  97.8 us (98%)
  local copies, waits for them, and re-layouts  1.3 us (1%)
    pallas_call x1, Pallas kernels, on_device(): pl.pallas_call(functools.partial(kernel, n_ep, chips, cap), out_shape=jax...  97.8 us

profile of v2, /device:TPU:65, one launch (start us, length us, event | category | flops | bytes accessed | tf_op | source)
XLA Modules:
  0.0 99.1 jit_solution(2009624057720428307)
XLA Ops:
  0.0 97.8 %shard_map.73 = bf16[32,128]{1,0:T(8,128)(2,1)} custom-call(bf16[32,128]{1,0:T(8,128)(2,1)} %tok_hbm.1, f32[16,128]{1,0:T(8,128)} %bitcast.3, s32[4,32]{1,0:T(4,128)} %bitcast.4, f32[4,32]{1,0:T(4,128)} %bitcast.5, bf16[1,2048,384]{2,1,0:T(8,128)(2,1)} %wg_hbm.1, bf16[1,2048,384]{2,1,0:T(8,128)(2,1)} %wu_hbm.1, bf16[1,384,2048]{2,1,0:T(8,128)(2,1)} %wd_hbm.1), custom_call_target="tpu_custom_call" | custom-call | tf_op jit(solution)/shard_map/pallas_call | solution.py:331
  97.8 1.3 %copy.9 = bf16[32,128]{1,0:T(8,128)(2,1)} copy(bf16[32,128]{1,0:T(8,128)(2,1)} %shard_map.73) | data formatting | bytes 16384

commit v3 on v1

--- a/solution.py
+++ b/solution.py
@@ -10,14 +10,9 @@
 MESH = pl.DeviceIdType.MESH
 epsilon = 1e-05
 CHIPS = 8
-CHUNKS = 2
-
-
-def ring_offsets(count):
-    offsets = [0]
-    for distance in range(1, count // 2):
-        offsets += [distance, -distance]
-    return offsets + [count // 2]
+CUTS = (0, 2, 8, 16)
+CHUNKS = len(CUTS) - 1
+DIRECT = (0,)
 
 
 def kernel(
@@ -37,11 +32,10 @@
     tok_rows, width = tok.shape
     top = routes.shape[0]
     hidden_units = w_own.shape[0]
-    offsets = ring_offsets(n_ep)
     all_rows = n_ep * cap
-    rows = all_rows // CHUNKS
-    half = rows // 2
-    slots = n_ep // CHUNKS
+    cuts = [cut * n_ep // CUTS[-1] for cut in CUTS]
+    firsts = [cut * cap for cut in cuts]
+    far_first = sorted(range(1, CHIPS), key=lambda d: -min(d, CHIPS - d))
 
     def chip(d):
         return lax.rem(x + d, CHIPS)
@@ -58,9 +52,9 @@
         return chip(d) * 2 + (core if p == 0 else 1 - core)
 
     barrier = pltpu.get_barrier_semaphore()
-    for offset in offsets[:0:-1]:
+    for offset in range(1, n_ep):
         pl.semaphore_signal(barrier, inc=1, device_id={"ep": ring(offset)}, device_id_type=MESH)
-    for d in (2, 6, 1, 7):
+    for d in far_first:
         pl.semaphore_signal(barrier, inc=1, device_id=at_chip(d), device_id_type=MESH)
     pl.semaphore_signal(barrier, inc=1, device_id=sibling, device_id_type=MESH)
 
@@ -110,7 +104,7 @@
     ).astype(jnp.bfloat16)
     packed[...] = outbox.reshape(n_ep, cap, width)
 
-    pl.semaphore_wait(barrier, (n_ep - 1) + 4 + 1)
+    pl.semaphore_wait(barrier, (n_ep - 1) + (CHIPS - 1) + 1)
 
     sent = []
 
@@ -123,17 +117,19 @@
         sent.append(copy)
         return copy
 
+    def landed(ref, semaphore):
+        pltpu.make_async_copy(ref, ref, semaphore).wait()
+
     def slot_rows(i):
-        return pl.ds(i * cap, cap)
-
-    dispatch = {}
-    for i in range(n_ep - 1, 0, -1):
-        expert = ring(-offsets[i])
-        dispatch[i] = send(
-            packed.at[expert], gathered.at[0, 0, slot_rows(i), :], z_send.at[i], z_recv.at[i],
+        return pl.ds(pl.multiple_of(i * cap, cap), cap)
+
+    for offset in sorted(range(1, n_ep), key=lambda o: -min(o, n_ep - o)):
+        expert = ring(offset)
+        send(
+            packed.at[expert], gathered.at[0, 0, slot_rows(z), :], z_send.at[offset], z_recv.at[z],
             {"ep": expert},
         )
-    gathered[0, 0, 0:cap, :] = packed[z]
+    gathered[0, 0, slot_rows(z), :] = packed[z]
 
     small[2].wait()
     mix = sum(
@@ -155,15 +151,18 @@
     mix_high, mix_low = flipped(mix_high), flipped(mix_low)
 
     def span(c):
-        return pl.ds(c * rows, rows)
+        return pl.ds(firsts[c], firsts[c + 1] - firsts[c])
+
+    def halved(c):
+        return (firsts[c + 1] - firsts[c]) // 2
 
     def top_half(c):
-        return pl.ds(c * rows, half)
+        return pl.ds(firsts[c], halved(c))
 
     def low_half(c):
-        return pl.ds(c * rows + half, half)
-
-    ag, d2d, halves, rs, back = {}, {}, {}, {}, {}
+        return pl.ds(firsts[c] + halved(c), halved(c))
+
+    ag, d2d, halves, rs = {}, {}, {}, {}
 
     def to_sibling(c, d, at, kind):
         d2d[c, kind] = send(
@@ -172,14 +171,27 @@
         )
 
     def gather_own(c):
-        for i in range(max(1, c * slots), (c + 1) * slots):
-            dispatch[i].wait_recv()
-        for kind, d, slot in ((2, 6, 2), (6, 2, 6), (1, 7, 1), (7, 1, 7)):
-            ag[c, kind] = send(
+        for s in range(cuts[c], cuts[c + 1]):
+
+            @pl.when(s != z)
+            def _():
+                landed(gathered.at[0, 0, slot_rows(s), :], z_recv.at[s])
+
+        if c in DIRECT:
+            hops = [(CHIPS - d, d) for d in far_first]
+        else:
+            hops = [(2, 6), (6, 2), (1, 7), (7, 1)]
+        for slot, d in hops:
+            ag[c, slot] = send(
                 gathered.at[0, 0, span(c), :], gathered.at[0, slot, span(c), :],
-                ag_send.at[c, kind], ag_recv.at[c, kind], at_chip(d),
+                ag_send.at[c, slot], ag_recv.at[c, slot], at_chip(d),
             )
         to_sibling(c, 0, span(c), 0)
+
+    def share(c):
+        for slot in (1, 7, 2, 6, 3, 5, 4):
+            ag[c, slot].wait_recv()
+            to_sibling(c, slot, span(c), slot)
 
     def gather_relay(c):
         for slot, near, far, opposite, at, kind in (
@@ -210,15 +222,16 @@
         to_sibling(c, 4, low_half(c), 8)
 
     def feed(c):
-        for kind in range(9):
+        for kind in range(8 if c in DIRECT else 9):
             d2d[c, kind].wait_recv()
         blocks = [(p, d) for p in range(2) for d in range(CHIPS)]
         features = len(blocks) * width
-        total = jnp.zeros((rows, width), jnp.float32)
+        shape = (firsts[c + 1] - firsts[c], width)
+        total = jnp.zeros(shape, jnp.float32)
         for p, d in blocks:
             total += gathered[p, d, span(c), :].astype(jnp.float32)
         average = jnp.sum(total, axis=1, keepdims=True) / features
-        total = jnp.zeros((rows, width), jnp.float32)
+        total = jnp.zeros(shape, jnp.float32)
         for p, d in blocks:
             off = gathered[p, d, span(c), :].astype(jnp.float32) - average
             total += off * off
@@ -239,80 +252,123 @@
         other = jnp.dot(hidden, w_other[...], preferred_element_type=jnp.float32)
         other = other.astype(jnp.bfloat16)
         for d in range(CHIPS):
-            part_out[c, d] = other[:, d * width : (d + 1) * width]
+            part_out[d, span(c), :] = other[:, d * width : (d + 1) * width]
         halves[c] = send(
-            part_out.at[c], part_in.at[c], half_send.at[c], half_recv.at[c], sibling
-        )
-        part_own[c] = jnp.dot(hidden, w_own[...], preferred_element_type=jnp.float32)
-
-    def chip_part(c, d):
-        return part_own[c, :, pl.ds(d * width, width)] + part_in[c, d].astype(jnp.float32)
-
-    def reduce_send(c, kind, d, source, slot, at=None):
-        src, dst = sums_out.at[c, source], sums_in.at[c, slot]
-        if at is not None:
-            src, dst = src.at[at, :], dst.at[at, :]
-        rs[c, kind] = send(src, dst, rs_send.at[c, kind], rs_recv.at[c, kind], at_chip(d))
+            part_out.at[:, span(c), :], part_in.at[:, span(c), :],
+            half_send.at[c], half_recv.at[c], sibling,
+        )
+        own = jnp.dot(hidden, w_own[...], preferred_element_type=jnp.float32)
+        for d in range(CHIPS):
+            part_own[d, span(c), :] = own[:, d * width : (d + 1) * width]
+
+    def serve(c):
+        feed(c)
+        project(c, expert(c))
+
+    def chip_part(d, at):
+        return part_own[d, at, :] + part_in[d, at, :].astype(jnp.float32)
+
+    def reduce_send(c, kind, d, source, slot, at):
+        rs[c, kind] = send(
+            sums_out.at[source, at, :], sums_in.at[slot, at, :],
+            rs_send.at[c, kind], rs_recv.at[c, kind], at_chip(d),
+        )
+
+    def reduce_direct(c):
+        halves[c].wait_recv()
+        for d in far_first:
+            sums_out[d, span(c), :] = chip_part(d, span(c)).astype(jnp.bfloat16)
+            reduce_send(c, CHIPS - d, d, d, CHIPS - d, span(c))
+
+    def finish_direct(c):
+        value = chip_part(0, span(c))
+        for slot in far_first:
+            rs[c, slot].wait_recv()
+            value += sums_in[slot, span(c), :].astype(jnp.float32)
+        give_back(c, value)
 
     def reduce_first(c):
         halves[c].wait_recv()
-        sums_out[c, 4] = chip_part(c, 4).astype(jnp.bfloat16)
-        reduce_send(c, 4, 2, 4, 4, pl.ds(0, half))
-        reduce_send(c, 0, 6, 4, 4, pl.ds(half, half))
+        sums_out[4, span(c), :] = chip_part(4, span(c)).astype(jnp.bfloat16)
+        reduce_send(c, 4, 2, 4, 4, top_half(c))
+        reduce_send(c, 0, 6, 4, 4, low_half(c))
         for d, near in ((3, 1), (5, 7), (1, 1), (7, 7)):
-            sums_out[c, d] = chip_part(c, d).astype(jnp.bfloat16)
-            reduce_send(c, d, near, d, d)
+            sums_out[d, span(c), :] = chip_part(d, span(c)).astype(jnp.bfloat16)
+            reduce_send(c, d, near, d, d, span(c))
 
     def reduce_second(c):
         rs[c, 4].wait_recv()
         rs[c, 0].wait_recv()
-        for d, near, at in ((2, 3, 0), (6, 5, half)):
+        for d, near, joined, alone in (
+            (2, 3, top_half(c), low_half(c)), (6, 5, low_half(c), top_half(c))
+        ):
             rs[c, near].wait_recv()
-            value = chip_part(c, d) + sums_in[c, near].astype(jnp.float32)
-            sums_out[c, d] = value.astype(jnp.bfloat16)
-            sums_out[c, d, pl.ds(at, half), :] = (
-                value[at : at + half] + sums_in[c, 4, pl.ds(at, half), :].astype(jnp.float32)
+            sums_out[d, joined, :] = (
+                chip_part(d, joined)
+                + sums_in[near, joined, :].astype(jnp.float32)
+                + sums_in[4, joined, :].astype(jnp.float32)
             ).astype(jnp.bfloat16)
-            reduce_send(c, d, d, d, d)
+            sums_out[d, alone, :] = (
+                chip_part(d, alone) + sums_in[near, alone, :].astype(jnp.float32)
+            ).astype(jnp.bfloat16)
+            reduce_send(c, d, d, d, d, span(c))
 
     def finish(c):
-        value = chip_part(c, 0)
+        value = chip_part(0, span(c))
         for slot in (1, 7, 2, 6):
             rs[c, slot].wait_recv()
-            value += sums_in[c, slot].astype(jnp.float32)
+            value += sums_in[slot, span(c), :].astype(jnp.float32)
+        give_back(c, value)
+
+    def back(s):
+        return pltpu.make_async_remote_copy(
+            src_ref=served.at[slot_rows(s), :], dst_ref=returned.at[z],
+            send_sem=back_send.at[s], recv_sem=back_recv.at[z],
+            device_id={"ep": s}, device_id_type=MESH,
+        )
+
+    def give_back(c, value):
         served[span(c), :] = value.astype(jnp.bfloat16)
-        for i in range((c + 1) * slots - 1, max(1, c * slots) - 1, -1):
-            back[i] = send(
-                served.at[slot_rows(i), :], returned.at[z], back_send.at[i], back_recv.at[i],
-                {"ep": ring(offsets[i])},
-            )
-        if c == 0:
-            returned[z] = served[0:cap, :]
+        for s in range(cuts[c], cuts[c + 1]):
+
+            @pl.when(s != z)
+            def _():
+                back(s).start()
+
+            @pl.when(s == z)
+            def _():
+                returned[z] = served[slot_rows(s), :]
 
     gather_own(0)
     gather_own(1)
-    gather_relay(0)
-    gather_relay(1)
-    gather_last(0)
+    gather_own(2)
     small[3].wait()
-    feed(0)
     pltpu.make_async_copy(w_in, w_in, in_sem).wait()
-    hidden = expert(0)
     pltpu.make_async_copy(w_other, w_other, other_sem).wait()
     pltpu.make_async_copy(w_own, w_own, own_sem).wait()
-    project(0, hidden)
+    share(0)
+    gather_relay(1)
+    serve(0)
+    gather_relay(2)
     gather_last(1)
-    reduce_first(0)
-    feed(1)
-    project(1, expert(1))
-    reduce_second(0)
+    reduce_direct(0)
+    serve(1)
+    gather_last(2)
     reduce_first(1)
-    finish(0)
+    serve(2)
+    finish_direct(0)
     reduce_second(1)
+    reduce_first(2)
     finish(1)
-
-    for i in range(n_ep - 1, 0, -1):
-        back[i].wait_recv()
+    reduce_second(2)
+    finish(2)
+
+    for e in range(n_ep):
+
+        @pl.when(e != z)
+        def _():
+            landed(returned.at[e], back_recv.at[e])
+
     values = returned[...].reshape(all_rows, width)
     out_ref[...] = (
         jnp.dot(mix_high, values, preferred_element_type=jnp.float32)
@@ -320,6 +376,11 @@
     ).astype(out_ref.dtype)
     for copy in sent:
         copy.wait_send()
+    for s in range(n_ep):
+
+        @pl.when(s != z)
+        def _():
+            back(s).wait_send()
 
 
 def solution(mesh):
@@ -331,7 +392,6 @@
         cap = min(tok_rows, 2 * tok_rows * top // n_ep)
         hidden_units = w_gate.shape[2]
         all_rows = n_ep * cap
-        rows = all_rows // CHUNKS
         features = n_tp * width
         bf16, f32 = jnp.bfloat16, jnp.float32
         dma = pltpu.SemaphoreType.DMA
@@ -351,11 +411,11 @@
                 pltpu.VMEM((n_ep, cap, width), bf16),
                 pltpu.VMEM((2, CHIPS, all_rows, width), bf16),
                 pltpu.VMEM((all_rows, features), bf16),
-                pltpu.VMEM((CHUNKS, rows, features // 2), f32),
-                pltpu.VMEM((CHUNKS, CHIPS, rows, width), bf16),
-                pltpu.VMEM((CHUNKS, CHIPS, rows, width), bf16),
-                pltpu.VMEM((CHUNKS, CHIPS, rows, width), bf16),
-                pltpu.VMEM((CHUNKS, CHIPS, rows, width), bf16),
+                pltpu.VMEM((CHIPS, all_rows, width), f32),
+                pltpu.VMEM((CHIPS, all_rows, width), bf16),
+                pltpu.VMEM((CHIPS, all_rows, width), bf16),
+                pltpu.VMEM((CHIPS, all_rows, width), bf16),
+                pltpu.VMEM((CHIPS, all_rows, width), bf16),
                 pltpu.VMEM((all_rows, width), bf16),
                 pltpu.VMEM((n_ep, cap, width), bf16),
                 dma((4,)), dma, dma, dma,

time: 89.5 us -> 84.7 us (0.946)
  Pallas kernels: 88 us -> 83.2 us
    pallas_call x1, Pallas kernels: 88 us -> 83.2 us  [on_device(): pl.pallas_call(functools.partial(kernel, n_ep, cap), out_shape=jax.ShapeD...]
where the time goes in v3:
time: 84.7 us; the launch traced here: 84.5 us
  Pallas kernels  83.2 us (98%)
  local copies, waits for them, and re-layouts  1.3 us (2%)
    pallas_call x1, Pallas kernels, on_device(): pl.pallas_call(functools.partial(kernel, n_ep, cap), out_shape=jax.ShapeD...  83.2 us

profile of v3, /device:TPU:80, one launch (start us, length us, event | category | flops | bytes accessed | tf_op | source)
XLA Modules:
  0.0 84.5 jit_solution(842476282276596045)
XLA Ops:
  0.0 83.2 %shard_map.73 = bf16[32,128]{1,0:T(8,128)(2,1)} custom-call(bf16[32,128]{1,0:T(8,128)(2,1)} %tok_hbm.1, f32[16,128]{1,0:T(8,128)} %bitcast.3, s32[4,32]{1,0:T(4,128)} %bitcast.4, f32[4,32]{1,0:T(4,128)} %bitcast.5, bf16[1,2048,384]{2,1,0:T(8,128)(2,1)} %wg_hbm.1, bf16[1,2048,384]{2,1,0:T(8,128)(2,1)} %wu_hbm.1, bf16[1,384,2048]{2,1,0:T(8,128)(2,1)} %wd_hbm.1), custom_call_target="tpu_custom_call" | custom-call | tf_op jit(solution)/shard_map/pallas_call | solution.py:398
  83.2 1.3 %copy.9 = bf16[32,128]{1,0:T(8,128)(2,1)} copy(bf16[32,128]{1,0:T(8,128)(2,1)} %shard_map.73) | data formatting | bytes 16384

commit v4 on v3

--- a/solution.py
+++ b/solution.py
@@ -10,9 +10,11 @@
 MESH = pl.DeviceIdType.MESH
 epsilon = 1e-05
 CHIPS = 8
-CUTS = (0, 2, 8, 16)
+ORDER = (0, 1, 2, 3, 4, 11, 12, 13, 5, 6, 9, 10, 7, 8, 14, 15)
+CUTS = (0, 2, 8, 12, 16)
 CHUNKS = len(CUTS) - 1
 DIRECT = (0,)
+LATE = 2
 
 
 def kernel(
@@ -21,7 +23,7 @@
     out_ref,
     tok, gain, routes, weights, w_in, w_own, w_other,
     packed, gathered, rows_in, part_own, part_out, part_in, sums_out, sums_in, served, returned,
-    small_sem, in_sem, own_sem, other_sem,
+    small_sem, in_sem, own_sem, other_sem, ready,
     z_send, z_recv, ag_send, ag_recv, d2d_send, d2d_recv, half_send, half_recv,
     rs_send, rs_recv, back_send, back_recv,
 ):
@@ -33,8 +35,8 @@
     top = routes.shape[0]
     hidden_units = w_own.shape[0]
     all_rows = n_ep * cap
-    cuts = [cut * n_ep // CUTS[-1] for cut in CUTS]
-    firsts = [cut * cap for cut in cuts]
+    firsts = [cut * cap for cut in CUTS]
+    early_count = n_ep - LATE
     far_first = sorted(range(1, CHIPS), key=lambda d: -min(d, CHIPS - d))
 
     def chip(d):
@@ -43,20 +45,25 @@
     def at_chip(d):
         return {"tp": chip(d) * 2 + core}
 
-    def ring(offset):
-        return lax.rem(z + offset + n_ep, n_ep)
-
     sibling = {"tp": x * 2 + 1 - core}
 
     def owner(p, d):
         return chip(d) * 2 + (core if p == 0 else 1 - core)
 
     barrier = pltpu.get_barrier_semaphore()
-    for offset in range(1, n_ep):
-        pl.semaphore_signal(barrier, inc=1, device_id={"ep": ring(offset)}, device_id_type=MESH)
+
+    def greet(device):
+        pl.semaphore_signal(barrier, inc=1, device_id=device, device_id_type=MESH)
+
+    for s in range(n_ep - 1, -1, -1):
+
+        @pl.when((s != z) & ((z < early_count) if s < early_count else (z >= 0)))
+        def _():
+            greet({"ep": s})
+
     for d in far_first:
-        pl.semaphore_signal(barrier, inc=1, device_id=at_chip(d), device_id_type=MESH)
-    pl.semaphore_signal(barrier, inc=1, device_id=sibling, device_id_type=MESH)
+        greet(at_chip(d))
+    greet(sibling)
 
     small = [
         pltpu.make_async_copy(source, target, small_sem.at[i])
@@ -104,9 +111,17 @@
     ).astype(jnp.bfloat16)
     packed[...] = outbox.reshape(n_ep, cap, width)
 
-    pl.semaphore_wait(barrier, (n_ep - 1) + (CHIPS - 1) + 1)
-
-    sent = []
+    @pl.when(z < early_count)
+    def _():
+        pl.semaphore_wait(barrier, early_count - 1 + CHIPS)
+
+    @pl.when(z >= early_count)
+    def _():
+        pl.semaphore_wait(barrier, n_ep - 1 + CHIPS)
+        for s in range(early_count):
+            pl.semaphore_signal(
+                ready.at[z - early_count], inc=1, device_id={"ep": s}, device_id_type=MESH
+            )
 
     def send(src, dst, send_sem, recv_sem, device):
         copy = pltpu.make_async_remote_copy(
@@ -114,22 +129,39 @@
             device_id=device, device_id_type=MESH,
         )
         copy.start()
-        sent.append(copy)
         return copy
 
     def landed(ref, semaphore):
         pltpu.make_async_copy(ref, ref, semaphore).wait()
 
-    def slot_rows(i):
+    def place_rows(i):
         return pl.ds(pl.multiple_of(i * cap, cap), cap)
 
-    for offset in sorted(range(1, n_ep), key=lambda o: -min(o, n_ep - o)):
-        expert = ring(offset)
-        send(
-            packed.at[expert], gathered.at[0, 0, slot_rows(z), :], z_send.at[offset], z_recv.at[z],
-            {"ep": expert},
-        )
-    gathered[0, 0, slot_rows(z), :] = packed[z]
+    my_place = sum(
+        ORDER.index(s) * (1 - (lax.rem(z - s + n_ep, n_ep) + n_ep - 1) // n_ep)
+        for s in range(n_ep)
+    )
+
+    def dispatch(s):
+        return pltpu.make_async_remote_copy(
+            src_ref=packed.at[s], dst_ref=gathered.at[0, 0, place_rows(my_place), :],
+            send_sem=z_send, recv_sem=z_recv.at[z],
+            device_id={"ep": s}, device_id_type=MESH,
+        )
+
+    for s in sorted(range(n_ep), key=lambda s: -min(s, n_ep - s)):
+
+        @pl.when((s != z) & ((z >= 0) if s < early_count else (z >= early_count)))
+        def _():
+            dispatch(s).start()
+
+    def dispatch_late(s):
+        @pl.when(z < early_count)
+        def _():
+            pl.semaphore_wait(ready.at[s - early_count], 1)
+            dispatch(s).start()
+
+    gathered[0, 0, place_rows(my_place), :] = packed[z]
 
     small[2].wait()
     mix = sum(
@@ -167,15 +199,15 @@
     def to_sibling(c, d, at, kind):
         d2d[c, kind] = send(
             gathered.at[0, d, at, :], gathered.at[1, d, at, :],
-            d2d_send.at[c, kind], d2d_recv.at[c, kind], sibling,
+            d2d_send.at[c], d2d_recv.at[c, kind], sibling,
         )
 
     def gather_own(c):
-        for s in range(cuts[c], cuts[c + 1]):
-
-            @pl.when(s != z)
+        for i in range(CUTS[c], CUTS[c + 1]):
+
+            @pl.when(ORDER[i] != z)
             def _():
-                landed(gathered.at[0, 0, slot_rows(s), :], z_recv.at[s])
+                landed(gathered.at[0, 0, place_rows(i), :], z_recv.at[ORDER[i]])
 
         if c in DIRECT:
             hops = [(CHIPS - d, d) for d in far_first]
@@ -184,7 +216,7 @@
         for slot, d in hops:
             ag[c, slot] = send(
                 gathered.at[0, 0, span(c), :], gathered.at[0, slot, span(c), :],
-                ag_send.at[c, slot], ag_recv.at[c, slot], at_chip(d),
+                ag_send.at[c], ag_recv.at[c, slot], at_chip(d),
             )
         to_sibling(c, 0, span(c), 0)
 
@@ -201,11 +233,11 @@
             ag[c, slot].wait_recv()
             ag[c, kind] = send(
                 gathered.at[0, slot, at, :], gathered.at[0, 4, at, :],
-                ag_send.at[c, kind], ag_recv.at[c, kind], at_chip(far),
+                ag_send.at[c], ag_recv.at[c, kind], at_chip(far),
             )
             ag[c, opposite] = send(
                 gathered.at[0, slot, span(c), :], gathered.at[0, opposite, span(c), :],
-                ag_send.at[c, opposite], ag_recv.at[c, opposite], at_chip(near),
+                ag_send.at[c], ag_recv.at[c, opposite], at_chip(near),
             )
             to_sibling(c, slot, span(c), slot)
         for slot in (1, 7):
@@ -271,7 +303,7 @@
     def reduce_send(c, kind, d, source, slot, at):
         rs[c, kind] = send(
             sums_out.at[source, at, :], sums_in.at[slot, at, :],
-            rs_send.at[c, kind], rs_recv.at[c, kind], at_chip(d),
+            rs_send.at[c], rs_recv.at[c, kind], at_chip(d),
         )
 
     def reduce_direct(c):
@@ -320,49 +352,65 @@
             value += sums_in[slot, span(c), :].astype(jnp.float32)
         give_back(c, value)
 
-    def back(s):
+    def back(i):
         return pltpu.make_async_remote_copy(
-            src_ref=served.at[slot_rows(s), :], dst_ref=returned.at[z],
-            send_sem=back_send.at[s], recv_sem=back_recv.at[z],
-            device_id={"ep": s}, device_id_type=MESH,
+            src_ref=served.at[place_rows(i), :], dst_ref=returned.at[z],
+            send_sem=back_send, recv_sem=back_recv.at[z],
+            device_id={"ep": ORDER[i]}, device_id_type=MESH,
         )
 
     def give_back(c, value):
         served[span(c), :] = value.astype(jnp.bfloat16)
-        for s in range(cuts[c], cuts[c + 1]):
-
-            @pl.when(s != z)
+        for i in range(CUTS[c], CUTS[c + 1]):
+
+            @pl.when(ORDER[i] != z)
             def _():
-                back(s).start()
-
-            @pl.when(s == z)
+                back(i).start()
+
+            @pl.when(ORDER[i] == z)
             def _():
-                returned[z] = served[slot_rows(s), :]
-
+                returned[z] = served[place_rows(i), :]
+
+    late = list(range(n_ep - 1, early_count - 1, -1))
     gather_own(0)
+    dispatch_late(late[0])
     gather_own(1)
+    dispatch_late(late[1])
     gather_own(2)
+    gather_own(3)
+    share(0)
     small[3].wait()
     pltpu.make_async_copy(w_in, w_in, in_sem).wait()
     pltpu.make_async_copy(w_other, w_other, other_sem).wait()
     pltpu.make_async_copy(w_own, w_own, own_sem).wait()
-    share(0)
+    serve(0)
     gather_relay(1)
-    serve(0)
+    reduce_direct(0)
     gather_relay(2)
+    gather_relay(3)
     gather_last(1)
-    reduce_direct(0)
     serve(1)
     gather_last(2)
+    gather_last(3)
+    finish_direct(0)
     reduce_first(1)
     serve(2)
-    finish_direct(0)
+    reduce_first(2)
+    serve(3)
     reduce_second(1)
-    reduce_first(2)
+    reduce_first(3)
+    reduce_second(2)
     finish(1)
-    reduce_second(2)
+    reduce_second(3)
     finish(2)
-
+    finish(3)
+
+    landed(packed.at[1:], z_send)
+    for c in range(CHUNKS):
+        landed(gathered.at[0, 1:, span(c), :], ag_send.at[c])
+        landed(gathered.at[0, :, span(c), :], d2d_send.at[c])
+        landed(part_out.at[:, span(c), :], half_send.at[c])
+        landed(sums_out.at[1:, span(c), :], rs_send.at[c])
     for e in range(n_ep):
 
         @pl.when(e != z)
@@ -374,13 +422,7 @@
         jnp.dot(mix_high, values, preferred_element_type=jnp.float32)
         + jnp.dot(mix_low, values, preferred_element_type=jnp.float32)
     ).astype(out_ref.dtype)
-    for copy in sent:
-        copy.wait_send()
-    for s in range(n_ep):
-
-        @pl.when(s != z)
-        def _():
-            back(s).wait_send()
+    landed(served.at[pl.ds(cap, all_rows - cap), :], back_send)
 
 
 def solution(mesh):
@@ -397,7 +439,7 @@
         dma = pltpu.SemaphoreType.DMA
         return pl.pallas_call(
             functools.partial(kernel, n_ep, cap),
-            out_shape=jax.ShapeDtypeStruct((tok_rows, width), bf16),
+            out_shape=pltpu.VMEM((tok_rows, width), bf16),
             in_specs=[pl.BlockSpec(memory_space=pltpu.HBM)] * 7,
             out_specs=pl.BlockSpec(memory_space=pltpu.VMEM),
             scratch_shapes=[
@@ -418,13 +460,13 @@
                 pltpu.VMEM((CHIPS, all_rows, width), bf16),
                 pltpu.VMEM((all_rows, width), bf16),
                 pltpu.VMEM((n_ep, cap, width), bf16),
-                dma((4,)), dma, dma, dma,
-                dma((n_ep,)), dma((n_ep,)),
-                dma((CHUNKS, 8)), dma((CHUNKS, 8)),
-                dma((CHUNKS, 9)), dma((CHUNKS, 9)),
+                dma((4,)), dma, dma, dma, pltpu.SemaphoreType.REGULAR((LATE,)),
+                dma, dma((n_ep,)),
+                dma((CHUNKS,)), dma((CHUNKS, 8)),
+                dma((CHUNKS,)), dma((CHUNKS, 9)),
                 dma((CHUNKS,)), dma((CHUNKS,)),
-                dma((CHUNKS, 8)), dma((CHUNKS, 8)),
-                dma((n_ep,)), dma((n_ep,)),
+                dma((CHUNKS,)), dma((CHUNKS, 8)),
+                dma, dma((n_ep,)),
             ],
             compiler_params=pltpu.CompilerParams(collective_id=0, has_side_effects=True),
         )(tokens, gain.reshape(n_tp, width), routes.T, weights.T, w_gate, w_up, w_down)

time: 84.7 us -> 78.6 us (0.928); the launches traced: 84.5 us -> 77.4 us
  Pallas kernels: 83.2 us -> 76.8 us
    pallas_call x1, Pallas kernels: 83.2 us -> 76.8 us  [on_device(): pl.pallas_call(functools.partial(kernel, n_ep, cap), out_shape=pltpu.VMEM...]
where the time goes in v4:
time: 78.6 us; the launch traced here: 77.4 us
  Pallas kernels  76.8 us (98%)
    pallas_call x1, Pallas kernels, on_device(): pl.pallas_call(functools.partial(kernel, n_ep, cap), out_shape=pltpu.VMEM...  76.8 us

profile of v4, /device:TPU:80, one launch (start us, length us, event | category | flops | bytes accessed | tf_op | source)
XLA Modules:
  0.0 77.4 jit_solution(18429686089040543657)
XLA Ops:
  0.0 76.8 %shard_map.73 = bf16[32,128]{1,0:T(8,128)(2,1)S(1)} custom-call(bf16[32,128]{1,0:T(8,128)(2,1)} %tok_hbm.1, f32[16,128]{1,0:T(8,128)} %bitcast.3, s32[4,32]{1,0:T(4,128)} %bitcast.4, f32[4,32]{1,0:T(4,128)} %bitcast.5, bf16[1,2048,384]{2,1,0:T(8,128)(2,1)} %wg_hbm.1, bf16[1,2048,384]{2,1,0:T(8,128)(2,1)} %wu_hbm.1, bf16[1,384,2048]{2,1,0:T(8,128)(2,1)} %wd_hbm.1), custom_call_target="tpu_custom_call" | custom-call | tf_op jit(solution)/shard_map/pallas_call | solution.py:440
  76.8 0.6 copy.9

commit v5 on v4

--- a/solution.py
+++ b/solution.py
@@ -10,11 +10,11 @@
 MESH = pl.DeviceIdType.MESH
 epsilon = 1e-05
 CHIPS = 8
-ORDER = (0, 1, 2, 3, 4, 11, 12, 13, 5, 6, 9, 10, 7, 8, 14, 15)
-CUTS = (0, 2, 8, 12, 16)
+ORDER = (0, 1, 2, 3, 4, 5, 11, 12, 13, 14, 15, 6, 7, 8, 9, 10)
+CUTS = (0, 3, 11, 16)
 CHUNKS = len(CUTS) - 1
 DIRECT = (0,)
-LATE = 2
+LATE = 1
 
 
 def kernel(
@@ -42,8 +42,10 @@
     def chip(d):
         return lax.rem(x + d, CHIPS)
 
+    chip_at = [chip(d) * 2 + core for d in range(CHIPS)]
+
     def at_chip(d):
-        return {"tp": chip(d) * 2 + core}
+        return {"tp": chip_at[d]}
 
     sibling = {"tp": x * 2 + 1 - core}
 
@@ -55,15 +57,25 @@
     def greet(device):
         pl.semaphore_signal(barrier, inc=1, device_id=device, device_id_type=MESH)
 
-    for s in range(n_ep - 1, -1, -1):
-
-        @pl.when((s != z) & ((z < early_count) if s < early_count else (z >= 0)))
+    far_offsets = sorted(range(1, n_ep), key=lambda o: -min(o, n_ep - o))
+    for offset in far_offsets:
+        s = lax.rem(z + offset, n_ep)
+
+        @pl.when((z < early_count) | (s >= early_count))
         def _():
             greet({"ep": s})
 
     for d in far_first:
         greet(at_chip(d))
     greet(sibling)
+
+    @pl.when(z >= early_count)
+    def _():
+        pl.semaphore_wait(barrier, n_ep - 1 + CHIPS)
+        for s in sorted(range(early_count), key=lambda s: min(s, n_ep - s)):
+            pl.semaphore_signal(
+                ready.at[z - early_count], inc=1, device_id={"ep": s}, device_id_type=MESH
+            )
 
     small = [
         pltpu.make_async_copy(source, target, small_sem.at[i])
@@ -73,23 +85,6 @@
     ]
     for copy in small:
         copy.start()
-    for p in range(2):
-        for d in range(CHIPS):
-            first = pl.multiple_of(owner(p, d) * width, width)
-            k = p * CHIPS + d
-            for j, source in enumerate((wg_hbm, wu_hbm)):
-                pltpu.make_async_copy(
-                    source.at[0, pl.ds(first, width), :],
-                    w_in.at[pl.ds(k * width, width), pl.ds(j * hidden_units, hidden_units)],
-                    in_sem,
-                ).start()
-    for p, target, sem in ((1, w_other, other_sem), (0, w_own, own_sem)):
-        for d in range(CHIPS):
-            first = pl.multiple_of(owner(p, d) * width, width)
-            pltpu.make_async_copy(
-                wd_hbm.at[0, :, pl.ds(first, width)], target.at[:, pl.ds(d * width, width)], sem
-            ).start()
-
     small[0].wait()
     small[1].wait()
     place = lax.broadcasted_iota(jnp.int32, (all_rows, tok_rows), 0)
@@ -115,14 +110,6 @@
     def _():
         pl.semaphore_wait(barrier, early_count - 1 + CHIPS)
 
-    @pl.when(z >= early_count)
-    def _():
-        pl.semaphore_wait(barrier, n_ep - 1 + CHIPS)
-        for s in range(early_count):
-            pl.semaphore_signal(
-                ready.at[z - early_count], inc=1, device_id={"ep": s}, device_id_type=MESH
-            )
-
     def send(src, dst, send_sem, recv_sem, device):
         copy = pltpu.make_async_remote_copy(
             src_ref=src, dst_ref=dst, send_sem=send_sem, recv_sem=recv_sem,
@@ -149,9 +136,10 @@
             device_id={"ep": s}, device_id_type=MESH,
         )
 
-    for s in sorted(range(n_ep), key=lambda s: -min(s, n_ep - s)):
-
-        @pl.when((s != z) & ((z >= 0) if s < early_count else (z >= early_count)))
+    for offset in far_offsets:
+        s = lax.rem(z + offset, n_ep)
+
+        @pl.when((z >= early_count) | (s < early_count))
         def _():
             dispatch(s).start()
 
@@ -162,6 +150,23 @@
             dispatch(s).start()
 
     gathered[0, 0, place_rows(my_place), :] = packed[z]
+
+    for p in range(2):
+        for d in range(CHIPS):
+            first = pl.multiple_of(owner(p, d) * width, width)
+            k = p * CHIPS + d
+            for j, source in enumerate((wg_hbm, wu_hbm)):
+                pltpu.make_async_copy(
+                    source.at[0, pl.ds(first, width), :],
+                    w_in.at[pl.ds(k * width, width), pl.ds(j * hidden_units, hidden_units)],
+                    in_sem,
+                ).start()
+    for p, target, sem in ((1, w_other, other_sem), (0, w_own, own_sem)):
+        for d in range(CHIPS):
+            first = pl.multiple_of(owner(p, d) * width, width)
+            pltpu.make_async_copy(
+                wd_hbm.at[0, :, pl.ds(first, width)], target.at[:, pl.ds(d * width, width)], sem
+            ).start()
 
     small[2].wait()
     mix = sum(
@@ -186,15 +191,15 @@
         return pl.ds(firsts[c], firsts[c + 1] - firsts[c])
 
     def halved(c):
-        return (firsts[c + 1] - firsts[c]) // 2
+        return ((CUTS[c + 1] - CUTS[c] + 1) // 2) * cap
 
     def top_half(c):
         return pl.ds(firsts[c], halved(c))
 
     def low_half(c):
-        return pl.ds(firsts[c] + halved(c), halved(c))
-
-    ag, d2d, halves, rs = {}, {}, {}, {}
+        return pl.ds(firsts[c] + halved(c), firsts[c + 1] - firsts[c] - halved(c))
+
+    ag, d2d, halves = {}, {}, {}
 
     def to_sibling(c, d, at, kind):
         d2d[c, kind] = send(
@@ -301,10 +306,13 @@
         return part_own[d, at, :] + part_in[d, at, :].astype(jnp.float32)
 
     def reduce_send(c, kind, d, source, slot, at):
-        rs[c, kind] = send(
+        send(
             sums_out.at[source, at, :], sums_in.at[slot, at, :],
             rs_send.at[c], rs_recv.at[c, kind], at_chip(d),
         )
+
+    def reduced(c, kind, at):
+        landed(sums_in.at[kind or 4, at, :], rs_recv.at[c, kind])
 
     def reduce_direct(c):
         halves[c].wait_recv()
@@ -315,7 +323,7 @@
     def finish_direct(c):
         value = chip_part(0, span(c))
         for slot in far_first:
-            rs[c, slot].wait_recv()
+            reduced(c, slot, span(c))
             value += sums_in[slot, span(c), :].astype(jnp.float32)
         give_back(c, value)
 
@@ -329,12 +337,12 @@
             reduce_send(c, d, near, d, d, span(c))
 
     def reduce_second(c):
-        rs[c, 4].wait_recv()
-        rs[c, 0].wait_recv()
+        reduced(c, 4, top_half(c))
+        reduced(c, 0, low_half(c))
         for d, near, joined, alone in (
             (2, 3, top_half(c), low_half(c)), (6, 5, low_half(c), top_half(c))
         ):
-            rs[c, near].wait_recv()
+            reduced(c, near, span(c))
             sums_out[d, joined, :] = (
                 chip_part(d, joined)
                 + sums_in[near, joined, :].astype(jnp.float32)
@@ -348,7 +356,7 @@
     def finish(c):
         value = chip_part(0, span(c))
         for slot in (1, 7, 2, 6):
-            rs[c, slot].wait_recv()
+            reduced(c, slot, span(c))
             value += sums_in[slot, span(c), :].astype(jnp.float32)
         give_back(c, value)
 
@@ -371,14 +379,12 @@
             def _():
                 returned[z] = served[place_rows(i), :]
 
-    late = list(range(n_ep - 1, early_count - 1, -1))
     gather_own(0)
-    dispatch_late(late[0])
+    for s in range(n_ep - 1, early_count - 1, -1):
+        dispatch_late(s)
     gather_own(1)
-    dispatch_late(late[1])
+    share(0)
     gather_own(2)
-    gather_own(3)
-    share(0)
     small[3].wait()
     pltpu.make_async_copy(w_in, w_in, in_sem).wait()
     pltpu.make_async_copy(w_other, w_other, other_sem).wait()
@@ -387,23 +393,18 @@
     gather_relay(1)
     reduce_direct(0)
     gather_relay(2)
-    gather_relay(3)
     gather_last(1)
     serve(1)
+    finish_direct(0)
     gather_last(2)
-    gather_last(3)
-    finish_direct(0)
-    reduce_first(1)
+    pl.when(core == 1)(lambda: reduce_first(1))
     serve(2)
+    pl.when(core == 0)(lambda: reduce_first(1))
     reduce_first(2)
-    serve(3)
     reduce_second(1)
-    reduce_first(3)
     reduce_second(2)
     finish(1)
-    reduce_second(3)
     finish(2)
-    finish(3)
 
     landed(packed.at[1:], z_send)
     for c in range(CHUNKS):

time: 78.6 us -> 78.8 us (level); the launches traced: 77.4 us -> 78.7 us
  Pallas kernels: 76.8 us -> 78.1 us
    pallas_call x1, Pallas kernels: 76.8 us -> 78.1 us  [on_device(): pl.pallas_call(functools.partial(kernel, n_ep, cap), out_shape=pltpu.VMEM...]
where the time goes in v5:
time: 78.8 us; the launch traced here: 78.7 us
  Pallas kernels  78.1 us (99%)
    pallas_call x1, Pallas kernels, on_device(): pl.pallas_call(functools.partial(kernel, n_ep, cap), out_shape=pltpu.VMEM...  78.1 us

profile of v5, /device:TPU:80, one launch (start us, length us, event | category | flops | bytes accessed | tf_op | source)
XLA Modules:
  0.0 78.7 jit_solution(10689815674645005374)
XLA Ops:
  0.0 78.1 %shard_map.73 = bf16[32,128]{1,0:T(8,128)(2,1)S(1)} custom-call(bf16[32,128]{1,0:T(8,128)(2,1)} %tok_hbm.1, f32[16,128]{1,0:T(8,128)} %bitcast.3, s32[4,32]{1,0:T(4,128)} %bitcast.4, f32[4,32]{1,0:T(4,128)} %bitcast.5, bf16[1,2048,384]{2,1,0:T(8,128)(2,1)} %wg_hbm.1, bf16[1,2048,384]{2,1,0:T(8,128)(2,1)} %wu_hbm.1, bf16[1,384,2048]{2,1,0:T(8,128)(2,1)} %wd_hbm.1), custom_call_target="tpu_custom_call" | custom-call | tf_op jit(solution)/shard_map/pallas_call | solution.py:441
  78.1 0.6 copy.9

commit v6 on v5

--- a/solution.py
+++ b/solution.py
@@ -10,8 +10,8 @@
 MESH = pl.DeviceIdType.MESH
 epsilon = 1e-05
 CHIPS = 8
-ORDER = (0, 1, 2, 3, 4, 5, 11, 12, 13, 14, 15, 6, 7, 8, 9, 10)
-CUTS = (0, 3, 11, 16)
+ORDER = (0, 1, 2, 3, 4, 11, 12, 13, 14, 5, 6, 7, 8, 9, 10, 15)
+CUTS = (0, 3, 9, 16)
 CHUNKS = len(CUTS) - 1
 DIRECT = (0,)
 LATE = 1
@@ -389,17 +389,16 @@
     pltpu.make_async_copy(w_in, w_in, in_sem).wait()
     pltpu.make_async_copy(w_other, w_other, other_sem).wait()
     pltpu.make_async_copy(w_own, w_own, own_sem).wait()
+    gather_relay(1)
     serve(0)
-    gather_relay(1)
     reduce_direct(0)
     gather_relay(2)
     gather_last(1)
     serve(1)
     finish_direct(0)
     gather_last(2)
-    pl.when(core == 1)(lambda: reduce_first(1))
+    reduce_first(1)
     serve(2)
-    pl.when(core == 0)(lambda: reduce_first(1))
     reduce_first(2)
     reduce_second(1)
     reduce_second(2)

time: 78.8 us -> 78.2 us (level)
  no operation moved by 1% of the time
where the time goes in v6:
time: 78.2 us; the launch traced here: 78 us
  Pallas kernels  77.4 us (99%)
    pallas_call x1, Pallas kernels, on_device(): pl.pallas_call(functools.partial(kernel, n_ep, cap), out_shape=pltpu.VMEM...  77.4 us

profile of v6, /device:TPU:80, one launch (start us, length us, event | category | flops | bytes accessed | tf_op | source)
XLA Modules:
  0.0 78.0 jit_solution(6367325580268908363)
XLA Ops:
  0.0 77.4 %shard_map.73 = bf16[32,128]{1,0:T(8,128)(2,1)S(1)} custom-call(bf16[32,128]{1,0:T(8,128)(2,1)} %tok_hbm.1, f32[16,128]{1,0:T(8,128)} %bitcast.3, s32[4,32]{1,0:T(4,128)} %bitcast.4, f32[4,32]{1,0:T(4,128)} %bitcast.5, bf16[1,2048,384]{2,1,0:T(8,128)(2,1)} %wg_hbm.1, bf16[1,2048,384]{2,1,0:T(8,128)(2,1)} %wu_hbm.1, bf16[1,384,2048]{2,1,0:T(8,128)(2,1)} %wd_hbm.1), custom_call_target="tpu_custom_call" | custom-call | tf_op jit(solution)/shard_map/pallas_call | solution.py:440
  77.4 0.6 copy.9

commit v7 on v6

--- a/solution.py
+++ b/solution.py
@@ -14,7 +14,7 @@
 CUTS = (0, 3, 9, 16)
 CHUNKS = len(CUTS) - 1
 DIRECT = (0,)
-LATE = 1
+LATE = 2
 
 
 def kernel(
@@ -389,8 +389,8 @@
     pltpu.make_async_copy(w_in, w_in, in_sem).wait()
     pltpu.make_async_copy(w_other, w_other, other_sem).wait()
     pltpu.make_async_copy(w_own, w_own, own_sem).wait()
+    serve(0)
     gather_relay(1)
-    serve(0)
     reduce_direct(0)
     gather_relay(2)
     gather_last(1)

time: 78.2 us -> 76.9 us (0.983); the launches traced: 78 us -> 75.5 us
  Pallas kernels: 77.4 us -> 74.9 us
    pallas_call x1, Pallas kernels: 77.4 us -> 74.9 us  [on_device(): pl.pallas_call(functools.partial(kernel, n_ep, cap), out_shape=pltpu.VMEM...]
where the time goes in v7:
time: 76.9 us; the launch traced here: 75.5 us
  Pallas kernels  74.9 us (97%)
    pallas_call x1, Pallas kernels, on_device(): pl.pallas_call(functools.partial(kernel, n_ep, cap), out_shape=pltpu.VMEM...  74.9 us

profile of v7, /device:TPU:80, one launch (start us, length us, event | category | flops | bytes accessed | tf_op | source)
XLA Modules:
  0.0 75.5 jit_solution(5200852987722351745)
XLA Ops:
  0.0 74.9 %shard_map.73 = bf16[32,128]{1,0:T(8,128)(2,1)S(1)} custom-call(bf16[32,128]{1,0:T(8,128)(2,1)} %tok_hbm.1, f32[16,128]{1,0:T(8,128)} %bitcast.3, s32[4,32]{1,0:T(4,128)} %bitcast.4, f32[4,32]{1,0:T(4,128)} %bitcast.5, bf16[1,2048,384]{2,1,0:T(8,128)(2,1)} %wg_hbm.1, bf16[1,2048,384]{2,1,0:T(8,128)(2,1)} %wu_hbm.1, bf16[1,384,2048]{2,1,0:T(8,128)(2,1)} %wd_hbm.1), custom_call_target="tpu_custom_call" | custom-call | tf_op jit(solution)/shard_map/pallas_call | solution.py:440
  74.9 0.6 copy.9
